TPU v7x, 32 devices: a whole 2x2x4 slice. The times are simulated.
32 devices in a mesh: fs: 8 (over z, y), tp: 4 (over x, core).
Axes of the slice: x: 2, y: 2, z: 4, core: 2. Of those that a mesh axis runs over, the one named last changes fastest.
Arguments:
- saved_inputs: bfloat16 [16384, 4096], P('fs'), may hold values from -6 to 6
- value_cot: bfloat16 [16384, 1024], P('fs', 'tp'), may hold values from -6 to 6
- gate_cot: bfloat16 [16384, 1024], P('fs', 'tp'), may hold values from -6 to 6
- point_inputs: bfloat16 [16384, 1024], P('fs'), may hold values from -6 to 6
- point_cot: bfloat16 [16384, 1024], P('fs', 'tp'), may hold values from -6 to 6
- master_value: float32 [4096, 1024], P('fs', 'tp'), may hold values from -6 to 6
- master_gate: float32 [4096, 1024], P('fs', 'tp'), may hold values from -6 to 6
- master_point: float32 [1024, 1024], P('fs', 'tp'), may hold values from -6 to 6
- factor_value: bfloat16 [4096, 256], P('fs'), may hold values from -160 to 160
- factor_gate: bfloat16 [4096, 256], P('fs'), may hold values from -160 to 160
- factor_point: bfloat16 [1024, 256], P('fs'), may hold values from -160 to 160
- first_value: float32 [256, 1024], P('fs', 'tp'), may hold values from -6 to 6
- first_gate: float32 [256, 1024], P('fs', 'tp'), may hold values from -6 to 6
- first_point: float32 [256, 1024], P('fs', 'tp'), may hold values from -6 to 6
- second_value: float32 [256, 1024], P('fs', 'tp'), may hold values from 0.2 to 2
- second_gate: float32 [256, 1024], P('fs', 'tp'), may hold values from 0.2 to 2
- second_point: float32 [256, 1024], P('fs', 'tp'), may hold values from 0.2 to 2
Outputs:
- new_value: float32 [4096, 1024], P('fs', 'tp')
- new_gate: float32 [4096, 1024], P('fs', 'tp')
- new_point: float32 [1024, 1024], P('fs', 'tp')
- copy_value: bfloat16 [4096, 1024], P(None, 'tp')
- copy_gate: bfloat16 [4096, 1024], P(None, 'tp')
- copy_point: bfloat16 [1024, 1024], P(None, 'tp')
- next_first_value: float32 [256, 1024], P('fs', 'tp')
- next_first_gate: float32 [256, 1024], P('fs', 'tp')
- next_first_point: float32 [256, 1024], P('fs', 'tp')
- next_second_value: float32 [256, 1024], P('fs', 'tp')
- next_second_gate: float32 [256, 1024], P('fs', 'tp')
- next_second_point: float32 [256, 1024], P('fs', 'tp')
All inputs are finite; a program needn't handle non-finite values.
Results may differ from a plain program's by a relative error of at most 0.0055.
Values may be sent and summed in bfloat16 or wider, within the bound.
A program may use at most 128 MiB of HBM per device.

v0:
```python
import jax
import jax.numpy as jnp
from jax import lax
from jax.sharding import PartitionSpec as P


def contract_rows(left, right):
    return lax.dot_general(
        left, right, (((0,), (0,)), ((), ())), preferred_element_type=jnp.float32
    )


def contract_split(projected, cot):
    upper = projected.astype(jnp.bfloat16)
    lower = (projected - upper.astype(jnp.float32)).astype(jnp.bfloat16)
    return contract_rows(upper, cot) + contract_rows(lower, cot)


def moments(low, first_old, second_old):
    first = 0.8 * first_old + 0.2 * low
    second = 0.9 * second_old + 0.1 * low * low
    return (first, second, first / (jnp.sqrt(second) + 1e-08))


def local(
    saved_inputs,
    value_cot,
    gate_cot,
    point_inputs,
    point_cot,
    master_value,
    master_gate,
    master_point,
    factor_value,
    factor_gate,
    factor_point,
    first_value,
    first_gate,
    first_point,
    second_value,
    second_gate,
    second_point,
):
    total = saved_inputs.shape[0] * lax.axis_size("fs")
    columns = saved_inputs
    proj_value = jnp.dot(
        columns,
        lax.all_gather(factor_value, "fs", axis=0, tiled=True),
        preferred_element_type=jnp.float32,
    )
    proj_gate = jnp.dot(
        columns,
        lax.all_gather(factor_gate, "fs", axis=0, tiled=True),
        preferred_element_type=jnp.float32,
    )
    columns = point_inputs
    proj_point = jnp.dot(
        columns,
        lax.all_gather(factor_point, "fs", axis=0, tiled=True),
        preferred_element_type=jnp.float32,
    )
    low_value = contract_split(proj_value, value_cot)
    low_gate = contract_split(proj_gate, gate_cot)
    low_point = contract_split(proj_point, point_cot)
    summed = (
        lax.psum_scatter(low_value, "fs", scatter_dimension=0, tiled=True),
        lax.psum_scatter(low_gate, "fs", scatter_dimension=0, tiled=True),
        lax.psum_scatter(low_point, "fs", scatter_dimension=0, tiled=True),
    )
    fv, sv, dv = moments(summed[0] / total, first_value, second_value)
    fg, sg, dg = moments(summed[1] / total, first_gate, second_gate)
    fpt, spt, dpt = moments(summed[2] / total, first_point, second_point)
    whole_v, whole_g, whole_p = (
        lax.all_gather(dv, "fs", axis=0, tiled=True),
        lax.all_gather(dg, "fs", axis=0, tiled=True),
        lax.all_gather(dpt, "fs", axis=0, tiled=True),
    )
    full_v = jnp.dot(factor_value.astype(jnp.float32), whole_v, precision=lax.Precision.HIGHEST)
    full_g = jnp.dot(factor_gate.astype(jnp.float32), whole_g, precision=lax.Precision.HIGHEST)
    full_p = jnp.dot(factor_point.astype(jnp.float32), whole_p, precision=lax.Precision.HIGHEST)
    squares = lax.psum(
        (jnp.sum(full_v * full_v), jnp.sum(full_g * full_g), jnp.sum(full_p * full_p)), ("fs", "tp")
    )
    spread = lax.axis_size("fs") * lax.axis_size("tp")
    entries_in = full_v.shape[0] * full_v.shape[1] * spread
    entries_point = full_p.shape[0] * full_p.shape[1] * spread
    new_v = master_value - 0.1 * lax.rsqrt(squares[0] / entries_in + 1e-06) * full_v
    new_g = master_gate - 0.1 * lax.rsqrt(squares[1] / entries_in + 1e-06) * full_g
    new_p = master_point - 0.1 * lax.rsqrt(squares[2] / entries_point + 1e-06) * full_p
    copy_v, copy_g, copy_p = (
        lax.all_gather(new_v.astype(jnp.bfloat16), "fs", axis=0, tiled=True),
        lax.all_gather(new_g.astype(jnp.bfloat16), "fs", axis=0, tiled=True),
        lax.all_gather(new_p.astype(jnp.bfloat16), "fs", axis=0, tiled=True),
    )
    return (new_v, new_g, new_p, copy_v, copy_g, copy_p, fv, fg, fpt, sv, sg, spt)


def solution(mesh):
    return jax.shard_map(
        local,
        mesh=mesh,
        in_specs=(
            P("fs", None),
            P("fs", "tp"),
            P("fs", "tp"),
            P("fs", None),
            P("fs", "tp"),
            P("fs", "tp"),
            P("fs", "tp"),
            P("fs", "tp"),
            P("fs", None),
            P("fs", None),
            P("fs", None),
            P("fs", "tp"),
            P("fs", "tp"),
            P("fs", "tp"),
            P("fs", "tp"),
            P("fs", "tp"),
            P("fs", "tp"),
        ),
        out_specs=(
            P("fs", "tp"),
            P("fs", "tp"),
            P("fs", "tp"),
            P(None, "tp"),
            P(None, "tp"),
            P(None, "tp"),
            P("fs", "tp"),
            P("fs", "tp"),
            P("fs", "tp"),
            P("fs", "tp"),
            P("fs", "tp"),
            P("fs", "tp"),
        ),
        check_vma=False,
    )
```

profile of v0, /device:TPU:0, one launch (start us, length us, event | category | flops | bytes accessed | tf_op | source)
XLA Modules:
  0.0 531.6 jit_solution(17776841322710641022)
XLA Ops:
  7.2 0.0 copy-start
  7.2 0.0 reduce-scatter.8.cloned.1.call-start
  7.2 33.4 %all_gather.31 = bf16[1024,256]{1,0:T(8,128)(2,1)S(1)} all-gather(bf16[128,256]{1,0:T(8,128)(2,1)} %param.27), channel_id=1, replica_groups=mesh['fs'=8,'tp'=4] {'fs'}, dimensions={0}, use_global_device_ids=true | all-gather | bytes 589824 | tf_op jit(solution)/shard_map/all_gather | solution.py:59
  40.6 3.5 fusion.14
  44.1 0.5 fusion.1
  44.6 0.0 copy-start.5
  44.6 0.0 copy-start.8
  44.6 0.0 copy-start.9
  44.6 1.2 convolution_add_fusion
  45.8 0.0 reduce-scatter.8.cloned.1.call-update
  45.8 0.0 all-gather.7.cloned.1.call-start
  45.9 0.7 all-gather.7.cloned.1.call-update
  46.6 0.0 all-gather.5.cloned.1.call-start
  46.6 0.7 all-gather.5.cloned.1.call-update
  47.3 0.0 reduce-scatter.6.cloned.1.call-start
  47.4 0.2 copy.29
  47.6 61.6 %reduce-scatter.8.cloned.1.call-done = f32[32,256]{1,0:T(8,128)} async-done(((f32[256,256]{1,0:T(8,128)}), f32[32,256]{1,0:T(8,128)}) %reduce-scatter.8.cloned.1.call-update) | async-done | bytes 32784 | tf_op jit(solution)/shard_map/reduce_scatter | solution.py:68
  109.2 1.4 add_divide_fusion
  110.6 31.4 %all_gather.32 = f32[256,256]{1,0:T(8,128)S(1)} all-gather(f32[32,256]{1,0:T(8,128)S(1)} %get-tuple-element.33), channel_id=1, replica_groups=mesh['fs'=8,'tp'=4] {'fs'}, dimensions={0}, use_global_device_ids=true | all-gather | bytes 294912 | tf_op jit(solution)/shard_map/all_gather | solution.py:76
  142.0 18.3 %all-gather.7.cloned.1.call-done = bf16[4096,256]{1,0:T(8,128)(2,1)} async-done(((bf16[512,256]{1,0:T(8,128)(2,1)}), bf16[4096,256]{1,0:T(8,128)(2,1)}) %all-gather.7.cloned.1.call-update) | async-done | bytes 2097168 | tf_op jit(solution)/shard_map/all_gather | solution.py:53
  160.3 8.7 %fusion.13 = f32[2048,256]{1,0:T(8,128)S(1)} fusion(bf16[2048,4096]{1,0:T(8,128)(2,1)} %param.17, bf16[4096,256]{1,0:T(8,128)(2,1)} %all-gather.7.cloned.1.call-done), kind=kOutput, calls=%fused_computation.34 | convolution fusion | flops 4294967296 | bytes 20971520 | tf_op jit(solution)/shard_map/dot_general | solution.py:51
  169.0 0.5 fusion.4
  169.5 1.2 convolution_add_fusion.1
  170.7 0.0 reduce-scatter.6.cloned.1.call-update
  170.7 0.0 copy-start.2
  170.7 0.0 reduce-scatter.4.cloned.1.call-start
  170.8 39.5 %all-gather.5.cloned.1.call-done = bf16[4096,256]{1,0:T(8,128)(2,1)} async-done(((bf16[512,256]{1,0:T(8,128)(2,1)}), bf16[4096,256]{1,0:T(8,128)(2,1)}) %all-gather.5.cloned.1.call-update) | async-done | bytes 2097168 | tf_op jit(solution)/shard_map/all_gather | solution.py:48
  210.3 8.7 %fusion.12 = f32[2048,256]{1,0:T(8,128)S(1)} fusion(bf16[2048,4096]{1,0:T(8,128)(2,1)} %param.17, bf16[4096,256]{1,0:T(8,128)(2,1)} %all-gather.5.cloned.1.call-done), kind=kOutput, calls=%fused_computation.33 | convolution fusion | flops 4294967296 | bytes 20971520 | tf_op jit(solution)/shard_map/dot_general | solution.py:46
  219.0 0.5 fusion.7
  219.5 0.0 copy-start.6
  219.5 0.0 copy-start.10
  219.5 0.0 copy-start.11
  219.5 0.0 copy-start.12
  219.5 0.0 copy-start.13
  219.6 0.0 copy-start.3
  219.6 1.2 convolution_add_fusion.2
  220.8 0.0 reduce-scatter.4.cloned.1.call-update
  220.8 0.0 all-gather.9.cloned.1.call-start
  220.9 1.0 multiply_reduce_fusion.2
  221.8 52.9 %reduce-scatter.6.cloned.1.call-done = f32[32,256]{1,0:T(8,128)} async-done(((f32[256,256]{1,0:T(8,128)}), f32[32,256]{1,0:T(8,128)}) %reduce-scatter.6.cloned.1.call-update) | async-done | bytes 32784 | tf_op jit(solution)/shard_map/reduce_scatter | solution.py:67
  274.7 1.4 add_divide_fusion.1
  276.1 30.9 %all_gather.30 = f32[256,256]{1,0:T(8,128)S(1)} all-gather(f32[32,256]{1,0:T(8,128)S(1)} %get-tuple-element.36), channel_id=1, replica_groups=mesh['fs'=8,'tp'=4] {'fs'}, dimensions={0}, use_global_device_ids=true | all-gather | bytes 294912 | tf_op jit(solution)/shard_map/all_gather | solution.py:75
  307.1 32.6 %reduce-scatter.4.cloned.1.call-done = f32[32,256]{1,0:T(8,128)} async-done(((f32[256,256]{1,0:T(8,128)}), f32[32,256]{1,0:T(8,128)}) %reduce-scatter.4.cloned.1.call-update) | async-done | bytes 32784 | tf_op jit(solution)/shard_map/reduce_scatter | solution.py:66
  339.6 1.4 add_divide_fusion.2
  341.0 30.8 %all_gather.28 = f32[256,256]{1,0:T(8,128)S(1)} all-gather(f32[32,256]{1,0:T(8,128)S(1)} %get-tuple-element.39), channel_id=1, replica_groups=mesh['fs'=8,'tp'=4] {'fs'}, dimensions={0}, use_global_device_ids=true | all-gather | bytes 294912 | tf_op jit(solution)/shard_map/all_gather | solution.py:74
  371.9 1.2 multiply_reduce_fusion.1
  373.1 1.2 multiply_reduce_fusion
  374.3 38.0 %all-reduce = (f32[]{:T(128)}, f32[]{:T(128)}, f32[]{:T(128)}) all-reduce(f32[]{:T(128)} %get-tuple-element.42, f32[]{:T(128)} %get-tuple-element.44, f32[]{:T(128)} %get-tuple-element.46), channel_id=1, replica_groups=mesh['fs'=8,'tp'=4] {'fs','tp'}, use_global_device_ids=true, to_apply=%region_2.0 | all-reduce | flops 3 | bytes 24 | tf_op jit(solution)/shard_map/psum | solution.py:81
  412.9 0.8 fusion.11
  413.7 0.0 all-gather.9.cloned.1.call-update
  413.8 0.0 all-gather.11.cloned.1.call-start
  413.8 1.2 copy.30
  415.7 0.8 fusion.10
  416.6 0.0 all-gather.11.cloned.1.call-update
  416.6 0.1 copy.31
  417.4 0.8 copy.34
  418.2 29.7 %all_gather.35 = bf16[1024,256]{0,1:T(8,128)(2,1)S(1)} all-gather(bf16[128,256]{0,1:T(8,128)(2,1)S(1)} %get-tuple-element.27), channel_id=1, replica_groups=mesh['fs'=8,'tp'=4] {'fs'}, dimensions={0}, use_global_device_ids=true | all-gather | bytes 589824 | tf_op jit(solution)/shard_map/all_gather | solution.py:93
  447.9 1.0 copy.37
  448.9 1.0 copy.32
  449.9 1.0 copy.33
  450.9 19.2 %all-gather.9.cloned.1.call-done = bf16[4096,256]{0,1:T(8,128)(2,1)} async-done(((bf16[512,256]{0,1:T(8,128)(2,1)}), bf16[4096,256]{0,1:T(8,128)(2,1)}) %all-gather.9.cloned.1.call-update) | async-done | bytes 2097168 | tf_op jit(solution)/shard_map/all_gather | solution.py:91
  470.1 4.1 copy.35
  474.2 46.5 %all-gather.11.cloned.1.call-done = bf16[4096,256]{0,1:T(8,128)(2,1)} async-done(((bf16[512,256]{0,1:T(8,128)(2,1)}), bf16[4096,256]{0,1:T(8,128)(2,1)}) %all-gather.11.cloned.1.call-update) | async-done | bytes 2097168 | tf_op jit(solution)/shard_map/all_gather | solution.py:92
  520.7 4.1 copy.36
  (18 shorter events, 0.1 us)
Async XLA Ops:
  7.2 36.9 %copy-start = (bf16[2048,256]{1,0:T(8,128)(2,1)S(1)}, bf16[2048,256]{1,0:T(8,128)(2,1)}, u32[]{:S(2)}) copy-start(bf16[2048,256]{1,0:T(8,128)(2,1)} %param.21) | copy-start | bytes 3145732
  7.2 102.0 %reduce-scatter.8.cloned.1.call-start = ((), (), s32[]{:S(2)}) async-start(), calls=%async_computation.7 | async-start | bytes 294912 | tf_op jit(solution)/shard_map/reduce_scatter | solution.py:68
  44.6 2.8 copy-start.5
  44.6 64.6 %copy-start.8 = (f32[32,256]{1,0:T(8,128)S(1)}, f32[32,256]{1,0:T(8,128)}, u32[]{:S(2)}) copy-start(f32[32,256]{1,0:T(8,128)} %param.33) | copy-start | bytes 98308
  44.6 64.6 %copy-start.9 = (f32[32,256]{1,0:T(8,128)S(1)}, f32[32,256]{1,0:T(8,128)}, u32[]{:S(2)}) copy-start(f32[32,256]{1,0:T(8,128)} %param.30) | copy-start | bytes 98308
  45.8 114.4 %all-gather.7.cloned.1.call-start = ((), (), s32[]{:S(2)}) async-start(), calls=%async_computation.5 | async-start | bytes 2359296 | tf_op jit(solution)/shard_map/all_gather | solution.py:53
  46.6 163.7 %all-gather.5.cloned.1.call-start = ((), (), s32[]{:S(2)}) async-start(), calls=%async_computation.3 | async-start | bytes 2359296 | tf_op jit(solution)/shard_map/all_gather | solution.py:48
  47.3 227.4 %reduce-scatter.6.cloned.1.call-start = ((), (), s32[]{:S(2)}) async-start(), calls=%async_computation.6 | async-start | bytes 294912 | tf_op jit(solution)/shard_map/reduce_scatter | solution.py:67
  142.0 27.0 %copy-start.1 = (bf16[2048,256]{1,0:T(8,128)(2,1)S(1)}, bf16[2048,256]{1,0:T(8,128)(2,1)}, u32[]{:S(2)}) copy-start(bf16[2048,256]{1,0:T(8,128)(2,1)} %param.19) | copy-start | bytes 3145732
  170.7 48.2 %copy-start.2 = (bf16[2048,256]{1,0:T(8,128)(2,1)S(1)}, bf16[2048,256]{1,0:T(8,128)(2,1)}, u32[]{:S(2)}) copy-start(bf16[2048,256]{1,0:T(8,128)(2,1)} %param.18) | copy-start | bytes 3145732
  170.7 168.9 %reduce-scatter.4.cloned.1.call-start = ((), (), s32[]{:S(2)}) async-start(), calls=%async_computation.4 | async-start | bytes 294912 | tf_op jit(solution)/shard_map/reduce_scatter | solution.py:66
  219.5 1.4 copy-start.6
  219.5 55.2 %copy-start.10 = (f32[32,256]{1,0:T(8,128)S(1)}, f32[32,256]{1,0:T(8,128)}, u32[]{:S(2)}) copy-start(f32[32,256]{1,0:T(8,128)} %param.32) | copy-start | bytes 98308
  219.5 55.2 %copy-start.11 = (f32[32,256]{1,0:T(8,128)S(1)}, f32[32,256]{1,0:T(8,128)}, u32[]{:S(2)}) copy-start(f32[32,256]{1,0:T(8,128)} %param.29) | copy-start | bytes 98308
  219.5 120.1 %copy-start.12 = (f32[32,256]{1,0:T(8,128)S(1)}, f32[32,256]{1,0:T(8,128)}, u32[]{:S(2)}) copy-start(f32[32,256]{1,0:T(8,128)} %param.31) | copy-start | bytes 98308
  219.5 120.1 %copy-start.13 = (f32[32,256]{1,0:T(8,128)S(1)}, f32[32,256]{1,0:T(8,128)}, u32[]{:S(2)}) copy-start(f32[32,256]{1,0:T(8,128)} %param.28) | copy-start | bytes 98308
  219.6 152.3 %copy-start.3 = (bf16[512,256]{1,0:T(8,128)(2,1)S(1)}, bf16[512,256]{1,0:T(8,128)(2,1)}, u32[]{:S(2)}) copy-start(bf16[512,256]{1,0:T(8,128)(2,1)} %param.25) | copy-start | bytes 786436
  220.8 152.3 %copy-start.4 = (bf16[512,256]{1,0:T(8,128)(2,1)S(1)}, bf16[512,256]{1,0:T(8,128)(2,1)}, u32[]{:S(2)}) copy-start(bf16[512,256]{1,0:T(8,128)(2,1)} %param.26) | copy-start | bytes 786436
  220.8 249.3 %all-gather.9.cloned.1.call-start = ((), (), s32[]{:S(2)}) async-start(), calls=%async_computation.8 | async-start | bytes 2359296 | tf_op jit(solution)/shard_map/all_gather | solution.py:91
  413.7 2.9 copy-start.7
  413.8 106.9 %all-gather.11.cloned.1.call-start = ((), (), s32[]{:S(2)}) async-start(), calls=%async_computation.9 | async-start | bytes 2359296 | tf_op jit(solution)/shard_map/all_gather | solution.py:92
Sparse Core Ops, SparseCore 0:
  46.0 63.1 reduce-scatter.7
  111.3 48.9 all-gather.6
  162.4 47.8 all-gather.4
  214.0 60.6 reduce-scatter.5
  278.5 61.1 reduce-scatter.3
  413.9 56.1 all-gather.8
  472.1 48.5 all-gather.10
where the time goes:
time: 532 us
  waiting for transfers between devices  272 us (51%)
  blocking collectives  194 us (36%)
  matrix products  29.3 us (6%)
  between operations  16.4 us (3%)
  local copies, waits for them, and re-layouts  13.5 us (3%)
  other arithmetic  5.86 us (1%)
    reduce_scatter x1, waiting for transfers between devices, local(): lax.psum_scatter(low_point, 'fs', scatter_dimension=0, tiled=True)  61.6 us
    reduce_scatter x1, waiting for transfers between devices, local(): lax.psum_scatter(low_gate, 'fs', scatter_dimension=0, tiled=True)  52.9 us
    all_gather x1, waiting for transfers between devices, local(): lax.all_gather(new_g.astype(jnp.bfloat16), 'fs', axis=0, tiled=True)  46.5 us
    all_gather x1, waiting for transfers between devices, local(): lax.all_gather(factor_value, 'fs', axis=0, tiled=True)  39.5 us
    psum x1, blocking collectives, local(): lax.psum((jnp.sum(full_v * full_v), jnp.sum(full_g * full_g), jnp.sum(ful...  38 us
    all_gather x1, blocking collectives, local(): lax.all_gather(factor_point, 'fs', axis=0, tiled=True)  33.4 us
    reduce_scatter x1, waiting for transfers between devices, local(): lax.psum_scatter(low_value, 'fs', scatter_dimension=0, tiled=True)  32.6 us
    all_gather x1, blocking collectives, local(): lax.all_gather(dpt, 'fs', axis=0, tiled=True)  31.4 us
  transfers between devices with their start and end apart: 7, of which 7 were waited for; matrix products, arithmetic and copies ran while one was open for 7% of the time, Pallas kernels for 0%

commit v1 on v0

--- a/solution.py
+++ b/solution.py
@@ -2,6 +2,18 @@
 import jax.numpy as jnp
 from jax import lax
 from jax.sharding import PartitionSpec as P
+
+
+def doubled_up(value, axis, dim):
+    ways, here = (lax.axis_size(axis), lax.axis_index(axis))
+    grown, reach = (value, 1)
+    while reach < ways:
+        theirs = lax.ppermute(grown, axis, [(d, d ^ reach) for d in range(ways)])
+        mine_first = jnp.concatenate([grown, theirs], axis=dim)
+        theirs_first = jnp.concatenate([theirs, grown], axis=dim)
+        grown = jnp.where(here & reach == 0, mine_first, theirs_first)
+        reach = 2 * reach
+    return grown
 
 
 def contract_rows(left, right):
@@ -73,7 +85,7 @@
     whole_v, whole_g, whole_p = (
         lax.all_gather(dv, "fs", axis=0, tiled=True),
         lax.all_gather(dg, "fs", axis=0, tiled=True),
-        lax.all_gather(dpt, "fs", axis=0, tiled=True),
+        doubled_up(dpt, "fs", 0),
     )
     full_v = jnp.dot(factor_value.astype(jnp.float32), whole_v, precision=lax.Precision.HIGHEST)
     full_g = jnp.dot(factor_gate.astype(jnp.float32), whole_g, precision=lax.Precision.HIGHEST)

time: 532 us -> 533 us (level)
  blocking collectives: 194 us -> 163 us
  waiting for transfers between devices: 272 us -> 300 us
    all_gather x1 -> x0, blocking collectives: 31.4 us -> none  [local(): lax.all_gather(dpt, 'fs', axis=0, tiled=True)]
    all_gather x1, waiting for transfers between devices: 18.3 us -> 40 us  [local(): lax.all_gather(factor_gate, 'fs', axis=0, tiled=True)]
    ppermute x0 -> x3, waiting for transfers between devices: none -> 6.57 us  [doubled_up(): theirs = lax.ppermute(grown, axis, [(d, d ^ reach) for d in range(ways)])]
    unnamed x37 -> x33, local copies, waits for them, and re-layouts: 13.5 us -> 13.5 us
  transfers between devices with their start and end apart: 7 -> 10, of which waited for: 7 -> 9; matrix products, arithmetic and copies ran while one was open for 7% -> 7% of each run, Pallas kernels for 0% -> 0%
where the time goes in v1:
time: 533 us; the launch traced here: 532 us
  waiting for transfers between devices  300 us (56%)
  blocking collectives  163 us (31%)
  matrix products  29.3 us (5%)
  between operations  16.4 us (3%)
  local copies, waits for them, and re-layouts  13.5 us (3%)
  other arithmetic  5.91 us (1%)
    reduce_scatter x1, waiting for transfers between devices, local(): lax.psum_scatter(low_point, 'fs', scatter_dimension=0, tiled=True)  61.8 us
    reduce_scatter x1, waiting for transfers between devices, local(): lax.psum_scatter(low_gate, 'fs', scatter_dimension=0, tiled=True)  52.9 us
    all_gather x1, waiting for transfers between devices, local(): lax.all_gather(new_g.astype(jnp.bfloat16), 'fs', axis=0, tiled=True)  46.5 us
    all_gather x1, waiting for transfers between devices, local(): lax.all_gather(factor_gate, 'fs', axis=0, tiled=True)  40 us
    all_gather x1, waiting for transfers between devices, local(): lax.all_gather(factor_value, 'fs', axis=0, tiled=True)  39.3 us
    psum x1, blocking collectives, local(): lax.psum((jnp.sum(full_v * full_v), jnp.sum(full_g * full_g), jnp.sum(ful...  37.8 us
    all_gather x1, blocking collectives, local(): lax.all_gather(factor_point, 'fs', axis=0, tiled=True)  33.4 us
    reduce_scatter x1, waiting for transfers between devices, local(): lax.psum_scatter(low_value, 'fs', scatter_dimension=0, tiled=True)  32.7 us
  transfers between devices with their start and end apart: 10, of which 9 were waited for; matrix products, arithmetic and copies ran while one was open for 7% of the time, Pallas kernels for 0%

profile of v1, /device:TPU:0, one launch (start us, length us, event | category | flops | bytes accessed | tf_op | source)
XLA Modules:
  0.0 532.1 jit_solution(13376494202518888004)
XLA Ops:
  7.2 0.0 copy-start
  7.2 0.0 reduce-scatter.8.cloned.1.call-start
  7.2 33.4 %all_gather.28 = bf16[1024,256]{1,0:T(8,128)(2,1)S(1)} all-gather(bf16[128,256]{1,0:T(8,128)(2,1)} %param.27), channel_id=1, replica_groups=mesh['fs'=8,'tp'=4] {'fs'}, dimensions={0}, use_global_device_ids=true | all-gather | bytes 589824 | tf_op jit(solution)/shard_map/all_gather | solution.py:71
  40.6 3.5 fusion.22
  44.1 0.5 fusion.1
  44.6 0.0 copy-start.8
  44.6 0.0 copy-start.9
  44.6 0.0 copy-start.5
  44.6 1.2 convolution_add_fusion
  45.8 0.0 reduce-scatter.8.cloned.1.call-update
  45.8 0.0 all-gather.7.cloned.1.call-start
  45.9 0.7 all-gather.7.cloned.1.call-update
  46.6 0.0 all-gather.5.cloned.1.call-start
  46.6 0.7 all-gather.5.cloned.1.call-update
  47.3 0.0 reduce-scatter.6.cloned.1.call-start
  47.4 61.8 %reduce-scatter.8.cloned.1.call-done = f32[32,256]{1,0:T(8,128)} async-done(((f32[256,256]{1,0:T(8,128)}), f32[32,256]{1,0:T(8,128)}) %reduce-scatter.8.cloned.1.call-update) | async-done | bytes 32784 | tf_op jit(solution)/shard_map/reduce_scatter | solution.py:80
  109.2 1.4 add_divide_fusion
  110.6 1.4 collective-permute-start
  112.0 2.5 collective-permute-done
  114.5 1.5 collective-permute-start.1
  116.0 0.2 copy.29
  116.2 4.0 collective-permute-done.1
  120.3 0.0 copy-start.1
  120.3 0.7 collective-permute-start.2
  121.0 40.0 %all-gather.7.cloned.1.call-done = bf16[4096,256]{1,0:T(8,128)(2,1)} async-done(((bf16[512,256]{1,0:T(8,128)(2,1)}), bf16[4096,256]{1,0:T(8,128)(2,1)}) %all-gather.7.cloned.1.call-update) | async-done | bytes 2097168 | tf_op jit(solution)/shard_map/all_gather | solution.py:65
  161.0 8.7 %fusion.21 = f32[2048,256]{1,0:T(8,128)S(1)} fusion(bf16[2048,4096]{1,0:T(8,128)(2,1)} %param.17, bf16[4096,256]{1,0:T(8,128)(2,1)} %all-gather.7.cloned.1.call-done), kind=kOutput, calls=%fused_computation.45 | convolution fusion | flops 4294967296 | bytes 20971520 | tf_op jit(solution)/shard_map/dot_general | solution.py:63
  169.7 0.5 fusion.4
  170.2 1.2 convolution_add_fusion.1
  171.4 0.0 reduce-scatter.6.cloned.1.call-update
  171.4 0.0 reduce-scatter.4.cloned.1.call-start
  171.5 39.3 %all-gather.5.cloned.1.call-done = bf16[4096,256]{1,0:T(8,128)(2,1)} async-done(((bf16[512,256]{1,0:T(8,128)(2,1)}), bf16[4096,256]{1,0:T(8,128)(2,1)}) %all-gather.5.cloned.1.call-update) | async-done | bytes 2097168 | tf_op jit(solution)/shard_map/all_gather | solution.py:60
  210.8 8.7 %fusion.20 = f32[2048,256]{1,0:T(8,128)S(1)} fusion(bf16[2048,4096]{1,0:T(8,128)(2,1)} %param.17, bf16[4096,256]{1,0:T(8,128)(2,1)} %all-gather.5.cloned.1.call-done), kind=kOutput, calls=%fused_computation.44 | convolution fusion | flops 4294967296 | bytes 20971520 | tf_op jit(solution)/shard_map/dot_general | solution.py:58
  219.5 0.5 fusion.7
  220.0 0.0 copy-start.11
  220.0 0.0 copy-start.3
  220.0 1.2 convolution_add_fusion.2
  221.2 0.0 reduce-scatter.4.cloned.1.call-update
  221.3 0.0 all-gather.9.cloned.1.call-start
  221.3 1.0 multiply_reduce_fusion.2
  222.3 52.9 %reduce-scatter.6.cloned.1.call-done = f32[32,256]{1,0:T(8,128)} async-done(((f32[256,256]{1,0:T(8,128)}), f32[32,256]{1,0:T(8,128)}) %reduce-scatter.6.cloned.1.call-update) | async-done | bytes 32784 | tf_op jit(solution)/shard_map/reduce_scatter | solution.py:79
  275.2 1.4 add_divide_fusion.1
  276.6 30.9 %all_gather.27 = f32[256,256]{1,0:T(8,128)S(1)} all-gather(f32[32,256]{1,0:T(8,128)S(1)} %get-tuple-element.36), channel_id=1, replica_groups=mesh['fs'=8,'tp'=4] {'fs'}, dimensions={0}, use_global_device_ids=true | all-gather | bytes 294912 | tf_op jit(solution)/shard_map/all_gather | solution.py:87
  307.5 32.7 %reduce-scatter.4.cloned.1.call-done = f32[32,256]{1,0:T(8,128)} async-done(((f32[256,256]{1,0:T(8,128)}), f32[32,256]{1,0:T(8,128)}) %reduce-scatter.4.cloned.1.call-update) | async-done | bytes 32784 | tf_op jit(solution)/shard_map/reduce_scatter | solution.py:78
  340.2 1.4 add_divide_fusion.2
  341.6 30.9 %all_gather.25 = f32[256,256]{1,0:T(8,128)S(1)} all-gather(f32[32,256]{1,0:T(8,128)S(1)} %get-tuple-element.39), channel_id=1, replica_groups=mesh['fs'=8,'tp'=4] {'fs'}, dimensions={0}, use_global_device_ids=true | all-gather | bytes 294912 | tf_op jit(solution)/shard_map/all_gather | solution.py:86
  372.5 1.2 multiply_reduce_fusion.1
  373.7 1.2 multiply_reduce_fusion
  374.9 37.8 %all-reduce = (f32[]{:T(128)}, f32[]{:T(128)}, f32[]{:T(128)}) all-reduce(f32[]{:T(128)} %get-tuple-element.42, f32[]{:T(128)} %get-tuple-element.44, f32[]{:T(128)} %get-tuple-element.46), channel_id=1, replica_groups=mesh['fs'=8,'tp'=4] {'fs','tp'}, use_global_device_ids=true, to_apply=%region_2.0 | all-reduce | flops 3 | bytes 24 | tf_op jit(solution)/shard_map/psum | solution.py:93
  413.4 0.8 fusion.19
  414.3 0.0 all-gather.9.cloned.1.call-update
  414.3 0.0 all-gather.11.cloned.1.call-start
  414.3 1.2 copy.30
  416.3 0.8 fusion.18
  417.1 0.0 all-gather.11.cloned.1.call-update
  417.1 0.1 copy.31
  418.0 0.8 copy.34
  418.7 29.6 %all_gather.31 = bf16[1024,256]{0,1:T(8,128)(2,1)S(1)} all-gather(bf16[128,256]{0,1:T(8,128)(2,1)S(1)} %get-tuple-element.27), channel_id=1, replica_groups=mesh['fs'=8,'tp'=4] {'fs'}, dimensions={0}, use_global_device_ids=true | all-gather | bytes 589824 | tf_op jit(solution)/shard_map/all_gather | solution.py:105
  448.3 1.0 copy.37
  449.3 1.0 copy.32
  450.3 1.0 copy.33
  451.3 19.3 %all-gather.9.cloned.1.call-done = bf16[4096,256]{0,1:T(8,128)(2,1)} async-done(((bf16[512,256]{0,1:T(8,128)(2,1)}), bf16[4096,256]{0,1:T(8,128)(2,1)}) %all-gather.9.cloned.1.call-update) | async-done | bytes 2097168 | tf_op jit(solution)/shard_map/all_gather | solution.py:103
  470.6 4.1 copy.35
  474.7 46.5 %all-gather.11.cloned.1.call-done = bf16[4096,256]{0,1:T(8,128)(2,1)} async-done(((bf16[512,256]{0,1:T(8,128)(2,1)}), bf16[4096,256]{0,1:T(8,128)(2,1)}) %all-gather.11.cloned.1.call-update) | async-done | bytes 2097168 | tf_op jit(solution)/shard_map/all_gather | solution.py:104
  521.2 4.1 copy.36
  (21 shorter events, 0.1 us)
Async XLA Ops:
  7.2 36.9 %copy-start = (bf16[2048,256]{1,0:T(8,128)(2,1)S(1)}, bf16[2048,256]{1,0:T(8,128)(2,1)}, u32[]{:S(2)}) copy-start(bf16[2048,256]{1,0:T(8,128)(2,1)} %param.21) | copy-start | bytes 3145732
  7.2 102.0 %reduce-scatter.8.cloned.1.call-start = ((), (), s32[]{:S(2)}) async-start(), calls=%async_computation.7 | async-start | bytes 294912 | tf_op jit(solution)/shard_map/reduce_scatter | solution.py:80
  44.6 64.6 %copy-start.8 = (f32[32,256]{1,0:T(8,128)S(1)}, f32[32,256]{1,0:T(8,128)}, u32[]{:S(2)}) copy-start(f32[32,256]{1,0:T(8,128)} %param.33) | copy-start | bytes 98308
  44.6 64.6 %copy-start.9 = (f32[32,256]{1,0:T(8,128)S(1)}, f32[32,256]{1,0:T(8,128)}, u32[]{:S(2)}) copy-start(f32[32,256]{1,0:T(8,128)} %param.30) | copy-start | bytes 98308
  44.6 71.4 %copy-start.5 = (f32[512,256]{1,0:T(8,128)S(1)}, f32[512,256]{1,0:T(8,128)}, u32[]{:S(2)}) copy-start(f32[512,256]{1,0:T(8,128)} %param.22) | copy-start | bytes 1572868
  45.8 115.1 %all-gather.7.cloned.1.call-start = ((), (), s32[]{:S(2)}) async-start(), calls=%async_computation.5 | async-start | bytes 2359296 | tf_op jit(solution)/shard_map/all_gather | solution.py:65
  46.6 164.1 %all-gather.5.cloned.1.call-start = ((), (), s32[]{:S(2)}) async-start(), calls=%async_computation.3 | async-start | bytes 2359296 | tf_op jit(solution)/shard_map/all_gather | solution.py:60
  47.3 227.8 %reduce-scatter.6.cloned.1.call-start = ((), (), s32[]{:S(2)}) async-start(), calls=%async_computation.6 | async-start | bytes 294912 | tf_op jit(solution)/shard_map/reduce_scatter | solution.py:79
  110.6 3.9 collective-permute-start
  114.5 5.7 %collective-permute-start.1 = (f32[64,256]{1,0:T(8,128)S(1)}, f32[64,256]{1,0:T(8,128)S(1)}, u32[]{:S(2)}, u32[]{:S(2)}) collective-permute-start(f32[64,256]{1,0:T(8,128)S(1)} %maximum_select_fusion.3), channel_id=1, source_target_pairs={{0,8},{4,12},{8,0},{12,4},{16,24},{20,28},{24,16},{28,20},{1,9},{5... | collective-permute-start | bytes 196616 | tf_op jit(solution)/shard_map/ppermute | solution.py:11
  120.3 49.4 %copy-start.1 = (bf16[2048,256]{1,0:T(8,128)(2,1)S(1)}, bf16[2048,256]{1,0:T(8,128)(2,1)}, u32[]{:S(2)}) copy-start(bf16[2048,256]{1,0:T(8,128)(2,1)} %param.19) | copy-start | bytes 3145732
  120.3 101.0 %collective-permute-start.2 = (f32[128,256]{1,0:T(8,128)S(1)}, f32[128,256]{1,0:T(8,128)S(1)}, u32[]{:S(2)}, u32[]{:S(2)}) collective-permute-start(f32[128,256]{1,0:T(8,128)S(1)} %maximum_select_fusion.2), channel_id=1, source_target_pairs={{0,16},{4,20},{8,24},{12,28},{16,0},{20,4},{24,8},{28,12},{1,17},{... | collective-permute-start | bytes 393224 | tf_op jit(solution)/shard_map/ppermute | solution.py:11
  171.4 48.1 %copy-start.2 = (bf16[2048,256]{1,0:T(8,128)(2,1)S(1)}, bf16[2048,256]{1,0:T(8,128)(2,1)}, u32[]{:S(2)}) copy-start(bf16[2048,256]{1,0:T(8,128)(2,1)} %param.18) | copy-start | bytes 3145732
  171.4 168.7 %reduce-scatter.4.cloned.1.call-start = ((), (), s32[]{:S(2)}) async-start(), calls=%async_computation.4 | async-start | bytes 294912 | tf_op jit(solution)/shard_map/reduce_scatter | solution.py:78
  220.0 1.3 copy-start.7
  220.0 55.2 %copy-start.10 = (f32[32,256]{1,0:T(8,128)S(1)}, f32[32,256]{1,0:T(8,128)}, u32[]{:S(2)}) copy-start(f32[32,256]{1,0:T(8,128)} %param.32) | copy-start | bytes 98308
  220.0 55.2 %copy-start.11 = (f32[32,256]{1,0:T(8,128)S(1)}, f32[32,256]{1,0:T(8,128)}, u32[]{:S(2)}) copy-start(f32[32,256]{1,0:T(8,128)} %param.29) | copy-start | bytes 98308
  220.0 152.5 %copy-start.3 = (bf16[512,256]{1,0:T(8,128)(2,1)S(1)}, bf16[512,256]{1,0:T(8,128)(2,1)}, u32[]{:S(2)}) copy-start(bf16[512,256]{1,0:T(8,128)(2,1)} %param.25) | copy-start | bytes 786436
  221.2 152.5 %copy-start.4 = (bf16[512,256]{1,0:T(8,128)(2,1)S(1)}, bf16[512,256]{1,0:T(8,128)(2,1)}, u32[]{:S(2)}) copy-start(bf16[512,256]{1,0:T(8,128)(2,1)} %param.26) | copy-start | bytes 786436
  221.3 249.3 %all-gather.9.cloned.1.call-start = ((), (), s32[]{:S(2)}) async-start(), calls=%async_computation.8 | async-start | bytes 2359296 | tf_op jit(solution)/shard_map/all_gather | solution.py:103
  414.3 2.9 copy-start.6
  414.3 106.9 %all-gather.11.cloned.1.call-start = ((), (), s32[]{:S(2)}) async-start(), calls=%async_computation.9 | async-start | bytes 2359296 | tf_op jit(solution)/shard_map/all_gather | solution.py:104
Sparse Core Ops, SparseCore 0:
  46.0 63.1 reduce-scatter.7
  111.3 49.6 all-gather.6
  163.1 47.6 all-gather.4
  214.5 60.6 reduce-scatter.5
  278.9 61.2 reduce-scatter.3
  414.4 56.1 all-gather.8
  472.6 48.5 all-gather.10
